TPU v7x, 32 devices: a whole 2x2x4 slice. The times are simulated.
32 devices in a mesh: ep: 8 (over z, core), tp: 4 (over y, x).
Axes of the slice: x: 2, y: 2, z: 4, core: 2. Of those that a mesh axis runs over, the one named last changes fastest.
Arguments:
- query_rows: bfloat16 [4096, 2048], P('ep', 'tp'), may hold values from -6 to 6
- key_rows: bfloat16 [4096, 2048], P('ep', 'tp'), may hold values from -6 to 6
- value_rows: bfloat16 [4096, 4096], P('ep', 'tp'), may hold values from -6 to 6
- in_gate: float32 [16, 4096], P('tp', 'ep'), may hold values from -120 to 120
- forget_gate: float32 [16, 4096], P('tp', 'ep'), may hold values from -2 to 20
- out_gate: bfloat16 [4096, 4096], P('ep', 'tp'), may hold values from -6 to 6
- head_gain: float32 [4096], P('tp'), may hold values from 0.1 to 1.9
- mix_weight: bfloat16 [4096, 4096], P(None, 'tp'), may hold values from -0.09375 to 0.09375
- expert_input: bfloat16 [2048, 4096], P('ep', 'tp'), may hold values from -30 to 30
- routes: int32 [2048, 2], P('ep'), may hold values from 0 to 7, all different within a row; in each aligned block of 256 rows (0 to 255, 256 to 511, ...) at most 128 rows name the same one
- route_weight: float32 [2048, 2], P('ep'), may hold values from 0.25 to 1.25
- gate_weight: bfloat16 [8, 1024, 4096], P('ep', 'tp'), may hold values from -0.09375 to 0.09375
- up_weight: bfloat16 [8, 1024, 4096], P('ep', 'tp'), may hold values from -0.09375 to 0.09375
- down_weight: bfloat16 [8, 1024, 4096], P('ep', None, 'tp'), may hold values from -0.1875 to 0.1875
Outputs:
- mixer_out: bfloat16 [4096, 4096], P('ep', 'tp')
- expert_out: bfloat16 [2048, 4096], P('ep', 'tp')
Inputs may be any that keep to these rules, and one draw needn't show every extreme that they name: `routes`: each row names 2 different experts. In the rows of one device no expert is named by more than 128 rows, and in the rows of some device an expert is named by exactly 128 rows.
All inputs are finite; a program needn't handle non-finite values.
Results may differ from a plain program's by a relative error of at most 0.0057.
Values may be sent and summed in bfloat16 or wider, within the bound.
A program may use at most 128 MiB of HBM per device.

v0:
```python
import jax
import jax.numpy as jnp
from jax import lax
from jax.sharding import PartitionSpec as P

D = 4096
BLOCK = 64


EPSILON = 1e-06
LOG_FLOOR = -1e30
HIGHEST_PRECISION = lax.Precision.HIGHEST


def carried_in(value, axis, join, neutral):
    count, mine = (lax.axis_size(axis), lax.axis_index(axis))
    pieces = jax.tree.map(lambda part: lax.all_gather(part, axis), value)
    subtotal = jax.tree.map(
        lambda part, zero: jnp.full_like(part, 0) + jnp.asarray(zero, part.dtype), value, neutral
    )

    def turn(position, subtotal):
        longer = join(subtotal, jax.tree.map(lambda part: part[position], pieces))
        return jax.tree.map(lambda new, old: jnp.where(position < mine, new, old), longer, subtotal)

    return lax.fori_loop(0, count - 1, turn, subtotal)


def combine(first_part, second_part):
    decay_first, max_first, memory_first, normal_first = first_part
    decay_second, max_second, memory_second, normal_second = second_part
    running_max = jnp.maximum(decay_second + max_first, max_second)
    keep_first = jnp.exp(decay_second + max_first - running_max)
    keep_second = jnp.exp(max_second - running_max)
    memory = (
        keep_first[..., None, None] * memory_first + keep_second[..., None, None] * memory_second
    )
    normalizer = keep_first[..., None] * normal_first + keep_second[..., None] * normal_second
    return (decay_first + decay_second, running_max, memory, normalizer)


def identity_state(head_count, key_width, value_width):
    return (
        jnp.zeros((head_count,), jnp.float32),
        jnp.full((head_count,), LOG_FLOOR, jnp.float32),
        jnp.zeros((head_count, key_width, value_width), jnp.float32),
        jnp.zeros((head_count, key_width), jnp.float32),
    )


def halfprod(form, left, right):
    return jnp.einsum(form, left, right, preferred_element_type=jnp.float32)


def prepare(query_heads, key_heads, value_heads, in_gate, forget_gate):
    head_count, length, key_width = query_heads.shape
    block_count = length // BLOCK
    query_blocks = query_heads.reshape(head_count, block_count, BLOCK, key_width)
    key_blocks = key_heads.reshape(head_count, block_count, BLOCK, key_width)
    value_blocks = value_heads.reshape(head_count, block_count, BLOCK, value_heads.shape[-1])
    log_input = in_gate.reshape(head_count, block_count, BLOCK)
    cumulative = jnp.cumsum(
        jax.nn.log_sigmoid(forget_gate).reshape(head_count, block_count, BLOCK), axis=-1
    )
    block_decay = cumulative[..., -1]
    weight_log = block_decay[..., None] - cumulative + log_input
    block_max = jnp.max(weight_log, axis=-1)
    weighted = (
        key_blocks.astype(jnp.float32) * jnp.exp(weight_log - block_max[..., None])[..., None]
    )
    normalizer = jnp.sum(weighted, axis=2)
    memory = halfprod("hcsk,hcsv->hckv", weighted.astype(jnp.bfloat16), value_blocks)
    return (
        (query_blocks, key_blocks, value_blocks, log_input, cumulative),
        (block_decay, block_max, memory, normalizer),
    )


def prefix(summary, initial):
    leading = jax.tree.map(lambda tensor: jnp.moveaxis(tensor, 1, 0), summary)

    def advance(running, current):
        return (combine(running, current), running)

    final_state, before = lax.scan(advance, initial, leading)
    return (final_state, jax.tree.map(lambda tensor: jnp.moveaxis(tensor, 0, 1), before))


def block_outputs(blocked, before):
    query_blocks, key_blocks, value_blocks, log_input, cumulative = blocked
    prior_max, prior_memory, prior_normal = (before[1], before[2], before[3])
    block_len = cumulative.shape[-1]
    scale = query_blocks.shape[-1] ** (-0.5)
    causal = jnp.tril(jnp.ones((block_len, block_len), dtype=bool))
    log_decay = jnp.where(
        causal,
        cumulative[..., :, None] - cumulative[..., None, :] + log_input[..., None, :],
        -jnp.inf,
    )
    log_inter = cumulative + prior_max[..., None]
    top_value = jnp.maximum(log_inter, jnp.max(log_decay, axis=-1))
    scores = (
        halfprod("hctk,hcsk->hcts", query_blocks, key_blocks)
        * scale
        * jnp.exp(log_decay - top_value[..., None])
    )
    carried = jnp.exp(log_inter - top_value) * scale
    query_wide = query_blocks.astype(jnp.float32)
    numerator = carried[..., None] * jnp.einsum(
        "hctk,hckv->hctv", query_wide, prior_memory, precision=HIGHEST_PRECISION
    ) + halfprod("hcts,hcsv->hctv", scores.astype(jnp.bfloat16), value_blocks)
    denominator = carried * jnp.einsum(
        "hctk,hck->hct", query_wide, prior_normal, precision=HIGHEST_PRECISION
    ) + jnp.sum(scores, axis=-1)
    return numerator / jnp.maximum(jnp.abs(denominator), jnp.exp(-top_value))[..., None]


def finish(head_values, out_gate, head_gain):
    head_count, block_count, block_len, value_width = head_values.shape
    per_head = jnp.transpose(head_values, (1, 2, 0, 3)).reshape(
        block_count * block_len, head_count, value_width
    )
    per_head = per_head * lax.rsqrt(jnp.mean(per_head * per_head, axis=-1, keepdims=True) + EPSILON)
    per_head = per_head.reshape(block_count * block_len, head_count * value_width) * head_gain
    per_head = per_head * jax.nn.sigmoid(out_gate.astype(jnp.float32))
    return per_head.astype(jnp.bfloat16)


def cell_heads(query_rows, key_rows, value_rows, in_gate, forget_gate, out_gate, head_gain):
    length = query_rows.shape[0]
    head_count = in_gate.shape[0]
    key_width = query_rows.shape[1] // head_count
    value_width = value_rows.shape[1] // head_count
    query_heads = query_rows.reshape(length, head_count, key_width).transpose(1, 0, 2)
    key_heads = key_rows.reshape(length, head_count, key_width).transpose(1, 0, 2)
    value_heads = value_rows.reshape(length, head_count, value_width).transpose(1, 0, 2)
    blocked, summary = prepare(query_heads, key_heads, value_heads, in_gate, forget_gate)
    initial = identity_state(head_count, key_width, value_width)
    final_state, before = prefix(summary, initial)
    incoming = carried_in(final_state, "ep", combine, initial)
    expanded = jax.tree.map(lambda tensor: tensor[:, None], incoming)
    before = combine(expanded, before)
    return finish(block_outputs(blocked, before), out_gate, head_gain)


def body(
    query_rows,
    key_rows,
    value_rows,
    in_gate,
    forget_gate,
    out_gate,
    head_gain,
    mix_weight,
    expert_input,
    routes,
    route_weight,
    gate_weight,
    up_weight,
    down_weight,
):
    mixed_heads = cell_heads(
        query_rows, key_rows, value_rows, in_gate, forget_gate, out_gate, head_gain
    )
    gate_local = gate_weight[0]
    up_local = up_weight[0]
    down_local = down_weight[0]
    group_size = lax.axis_size("ep")
    token_count, fanout = routes.shape
    capacity = 2 * token_count * fanout // group_size
    slot_count = group_size * capacity
    chosen = routes.reshape(-1)
    one_hot = (chosen[:, None] == jnp.arange(group_size, dtype=jnp.int32)[None, :]).astype(
        jnp.int32
    )
    position = jnp.sum((jnp.cumsum(one_hot, axis=0) - one_hot) * one_hot, axis=1)
    target = chosen * capacity + position
    matches = (jnp.arange(slot_count, dtype=jnp.int32)[:, None] == target[None, :]).astype(
        jnp.int32
    )
    occupied = jnp.sum(matches, axis=1) > 0
    source_row = jnp.sum(
        matches * (jnp.arange(token_count * fanout, dtype=jnp.int32) // fanout)[None, :], axis=1
    )
    arrived = lax.all_to_all(
        jnp.where(
            occupied[:, None],
            jnp.take(expert_input, source_row, axis=0),
            jnp.zeros((), expert_input.dtype),
        ),
        "ep",
        split_axis=0,
        concat_axis=0,
        tiled=True,
    )
    head_piece = lax.all_gather(mixed_heads, "tp", axis=1, tiled=True)
    token_piece = lax.all_gather(arrived, "tp", axis=1, tiled=True)
    mix_acc = jnp.dot(head_piece, mix_weight, preferred_element_type=jnp.float32)
    gate_acc = jnp.einsum("sd,fd->sf", token_piece, gate_local, preferred_element_type=jnp.float32)
    up_acc = jnp.einsum("sd,fd->sf", token_piece, up_local, preferred_element_type=jnp.float32)
    squares = jnp.sum(jnp.square(token_piece.astype(jnp.float32)), axis=1)
    mix_acc, gate_acc, up_acc, squares = (mix_acc, gate_acc, up_acc, squares)
    mixer_out = mix_acc.astype(jnp.bfloat16)
    inverse_rms = lax.rsqrt(squares / D + EPSILON)[:, None]
    hidden = (jax.nn.silu(gate_acc * inverse_rms) * (up_acc * inverse_rms)).astype(jnp.bfloat16)
    expert_rows = jnp.dot(
        lax.all_gather(hidden, "tp", axis=1, tiled=True),
        down_local,
        preferred_element_type=jnp.float32,
    )
    returned_rows = lax.all_to_all(
        expert_rows.astype(jnp.bfloat16), "ep", split_axis=0, concat_axis=0, tiled=True
    )
    picked_rows = (
        jnp.take(returned_rows, target, axis=0).reshape(token_count, fanout, -1).astype(jnp.float32)
    )
    expert_out = jnp.sum(picked_rows * route_weight[:, :, None], axis=1).astype(jnp.bfloat16)
    return (mixer_out, expert_out)


def solution(mesh):
    in_specs = (
        P("ep", "tp"),
        P("ep", "tp"),
        P("ep", "tp"),
        P("tp", "ep"),
        P("tp", "ep"),
        P("ep", "tp"),
        P("tp"),
        P(None, "tp"),
        P("ep", "tp"),
        P("ep", None),
        P("ep", None),
        P("ep", "tp", None),
        P("ep", "tp", None),
        P("ep", None, "tp"),
    )
    out_specs = (P("ep", "tp"), P("ep", "tp"))
    return jax.shard_map(body, mesh=mesh, in_specs=in_specs, out_specs=out_specs, check_vma=False)
```

profile of v0, /device:TPU:0, one launch (start us, length us, event | category | flops | bytes accessed | tf_op | source)
XLA Modules:
  0.0 351.7 jit_solution(7868608144681176539)
XLA Ops:
  10.5 2.6 reshape.229
  13.1 2.3 copy.78
  18.0 3.1 convolution_bitcast_fusion
  21.1 18.0 %while.43 = (s32[]{:T(128)}, f32[4]{0:T(128)S(1)}, f32[4]{0:T(128)S(1)}, f32[4,128,256]{2,1,0:T(8,128)S(1)}, f32[4,128]{1,0:T(4,128)S(1)}, /*index=5*/f32[8,4]{1...) while((s32[]{:T(128)}, f32[4]{0:T(128)S(1)}, ...), condition=%wide.region_4.5_spmd.clone, body=%wide.region_3.4_spmd.clone.sunk | while | flops 657951 | bytes 2636291 | solution.py:85
  42.6 5.4 %gather_fusion = bf16[1024,1024]{1,0:T(8,128)(2,1)} fusion(bf16[256,1024]{1,0:T(8,128)(2,1)S(1)} %copy-done.1, s32[1024]{0:T(1024)S(1)} %broadcast_clamp_fusion), kind=kCustom, calls=%fused_computation | custom fusion | bytes 4198400 | tf_op jit(solution)/shard_map/jit(_take)/gather | solution.py:188
  48.0 1.9 select_select_fusion
  49.9 83.4 %all_to_all.21 = bf16[8,128,1024]{2,1,0:T(8,128)(2,1)} all-to-all(bf16[8,128,1024]{2,1,0:T(8,128)(2,1)S(1)} %select_select_fusion), channel_id=1, replica_groups=mesh['ep'=8,'tp'=4] {'ep'}, dimensions={0} | all-to-all | bytes 4194304 | tf_op jit(solution)/shard_map/all_to_all | solution.py:185
  135.6 14.3 %all-reduce.2 = (f32[32]{0:T(128)S(1)}, f32[32]{0:T(128)S(1)}) all-reduce(f32[32]{0:T(128)S(1)} %dynamic-update-slice, f32[32]{0:T(128)S(1)} %dynamic-update-slice.1), channel_id=2, replica_groups=mesh['ep'=8,'tp'=4] {'ep'}, use_global_device_ids=true, to_apply=%add | all-reduce | flops 64 | bytes 512
  152.1 13.0 %all-gather.4 = f32[8,4,128]{2,1,0:T(4,128)S(1)} all-gather(f32[1,4,128]{2,1,0:T(4,128)S(1)} %bitcast.238), channel_id=5, replica_groups=mesh['ep'=8,'tp'=4] {'ep'}, dimensions={0}, use_global_device_ids=true | all-gather | bytes 18432 | tf_op jit(solution)/shard_map/all_gather | solution.py:17
  165.7 9.6 %while.44 = (s32[]{:T(128)}, f32[4]{0:T(128)S(1)}, f32[4,128,256]{2,1,0:T(8,128)S(1)}, f32[4,128]{1,0:T(4,128)S(1)}, s32[]{:T(128)}, /*index=5*/f32[8,4]{1,0:T(8...) while((s32[]{:T(128)}, f32[4]{0:T(128)S(1)}, ...), condition=%wide.region_6.7_spmd.clone, body=%wide.region_5.6_spmd.clone.sunk | while | flops 657956 | bytes 1579390 | solution.py:26
  175.4 44.2 %all-gather.12.cloned.1.call-done = bf16[1024,4096]{1,0:T(8,128)(2,1)} async-done(((bf16[1024,1024]{1,0:T(8,128)(2,1)}), bf16[1024,4096]{1,0:T(8,128)(2,1)}) %all-gather.12.cloned.1.call-update) | async-done | bytes 8388624 | tf_op jit(solution)/shard_map/all_gather | solution.py:197
  219.6 5.2 %multiply_reduce_fusion = f32[1024]{0:T(1024)S(1)} fusion(bf16[1024,4096]{1,0:T(8,128)(2,1)} %all-gather.12.cloned.1.call-done), kind=kLoop, calls=%fused_computation.36 | loop fusion | flops 12581888 | bytes 8392704 | tf_op jit(solution)/shard_map/reduce_sum | solution.py:201
  225.4 4.1 %fusion.29 = f32[1024,256]{1,0:T(8,128)S(1)} fusion(bf16[1024,4096]{1,0:T(8,128)(2,1)S(1)} %copy-done.3, bf16[1,256,4096]{2,1,0:T(8,128)(2,1)} %param.29, f32[1024]{0:T(1024)S(1)} %add_rsqrt_fusion.1), kind=kOutput, calls=%fused_computation.63 | convolution fusion | flops 2147745792 | bytes 11538432 | tf_op jit(solution)/shard_map/sd,fd->sf/dot_general | solution.py:199
  229.5 3.3 fusion.38
  234.2 1.7 fusion.65
  236.0 4.4 %fusion.16 = f32[4,8,256,64]{2,3,1,0:T(8,128)S(1)} fusion(bf16[4,8,64,128]{3,2,1,0:T(8,128)(2,1)S(1)} %bitcast.231, f32[8,4,128,256]{3,2,1,0:T(8,128)} %get-tuple-element.240, f32[4,8]{0,1:T(8,128)S(1)} %fusion.58, f32[4,128,256]{2,1,0:T(8,128)S(1)} %get-tuple-element.239, f32[4,8]{0,1:T(8,128)S(1)} %get-tuple-element.432), kind=kOutput, calls=%fused_computation.39 | convolution fusion | flops 808452096 | bytes 7340288 | tf_op jit(solution)/shard_map/hctk,hckv->hctv/dot_general | solution.py:109
  243.5 1.8 copy.102
  249.6 18.4 %all-gather.14.cloned.1.call-done = bf16[1024,1024]{1,0:T(8,128)(2,1)} async-done(((bf16[1024,256]{1,0:T(8,128)(2,1)}), bf16[1024,1024]{1,0:T(8,128)(2,1)}) %all-gather.14.cloned.1.call-update) | async-done | bytes 2097168 | tf_op jit(solution)/shard_map/all_gather | solution.py:207
  268.0 5.3 %fusion.25 = bf16[1024,1024]{1,0:T(8,128)(2,1)} fusion(bf16[1024,1024]{1,0:T(8,128)(2,1)} %all-gather.14.cloned.1.call-done, bf16[1,1024,1024]{2,1,0:T(8,128)(2,1)S(1)} %copy-done), kind=kOutput, calls=%fused_computation.59 | convolution fusion | flops 2148532224 | bytes 6291456 | tf_op jit(solution)/shard_map/dot_general | solution.py:206
  273.3 4.7 %all-to-all-start.1 = ((bf16[8,128,1024]{2,1,0:T(8,128)(2,1)}), bf16[8,128,1024]{2,1,0:T(8,128)(2,1)}, u32[]{:S(2)}, u32[]{:S(2)}) async-start(bf16[8,128,1024]{2,1,0:T(8,128)(2,1)} %bitcast.232), calls=%async_computation.1 | async-start | bytes 4194304 | tf_op jit(solution)/shard_map/all_to_all | solution.py:211
  278.9 44.0 %all-gather.10.cloned.1.call-done = bf16[512,4096]{1,0:T(8,128)(2,1)} async-done(((bf16[512,1024]{1,0:T(8,128)(2,1)}), bf16[512,4096]{1,0:T(8,128)(2,1)}) %all-gather.10.cloned.1.call-update) | async-done | bytes 4194320 | tf_op jit(solution)/shard_map/all_gather | solution.py:196
  322.9 10.1 %convolution_convert_fusion = bf16[512,1024]{1,0:T(8,128)(2,1)} fusion(bf16[512,4096]{1,0:T(8,128)(2,1)} %all-gather.10.cloned.1.call-done, bf16[4096,1024]{1,0:T(8,128)(2,1)} %param.25), kind=kOutput, calls=%fused_computation.60 | convolution fusion | flops 4295491584 | bytes 13631488 | tf_op jit(solution)/shard_map/dot_general | solution.py:198
  333.0 4.6 %gather_fusion.1 = bf16[512,1024]{1,0:T(8,128)(2,1)S(1)} fusion(bf16[1024,1024]{1,0:T(8,128)(2,1)} %bitcast.39, s32[1024]{0:T(1024)S(1)} %pad_clamp_fusion), kind=kCustom, calls=%fused_computation.1 | custom fusion | bytes 2099200 | tf_op jit(solution)/shard_map/jit(_take)/gather | solution.py:215
  338.8 6.3 %multiply_reduce_fusion.1 = bf16[256,1024]{1,0:T(8,128)(2,1)} fusion(bf16[256,2,1024]{2,1,0:T(2,128)(2,1)} %gather.15, pred[256,2]{1,0:T(8,128)(4,1)S(1)} %copy.93, f32[256,2]{1,0:T(8,128)S(1)} %copy.95), kind=kLoop, calls=%fused_computation.51 | loop fusion | flops 1835008 | bytes 1575424 | tf_op jit(solution)/shard_map/reduce_sum | solution.py:217
  (217 shorter events, 52.4 us)
Async XLA Ops:
  7.2 260.8 %copy-start = (bf16[1,1024,1024]{2,1,0:T(8,128)(2,1)S(1)}, bf16[1,1024,1024]{2,1,0:T(8,128)(2,1)}, u32[]{:S(2)}) copy-start(bf16[1,1024,1024]{2,1,0:T(8,128)(2,1)} %param.31) | copy-start | bytes 6291460
  7.2 158.5 %all-gather.16.cloned.1.call-start = ((), (), s32[]{:S(2)}) async-start(), calls=%async_computation.5 | async-start | bytes 4718592 | tf_op jit(solution)/shard_map/all_gather | solution.py:17
  16.6 1.4 copy-start.5
  16.7 4.4 %copy-start.7 = (bf16[4,512,128]{2,1,0:T(8,128)(2,1)}, bf16[4,512,128]{2,1,0:T(8,128)(2,1)S(1)}, u32[]{:S(2)}) copy-start(bf16[4,512,128]{2,1,0:T(8,128)(2,1)S(1)} %copy.77) | copy-start | bytes 1572868
  21.1 18.9 %copy-start.10 = (s32[256,2]{0,1:T(2,128)S(1)}, s32[256,2]{0,1:T(2,128)}, u32[]{:S(2)}) copy-start(s32[256,2]{0,1:T(2,128)} %param.27) | copy-start | bytes 6148
  39.1 0.8 copy-start.2
  39.2 3.5 copy-start.1
  40.0 179.6 %all-gather.12.cloned.1.call-start = ((), (), s32[]{:S(2)}) async-start(), calls=%async_computation.3 | async-start | bytes 10485760 | tf_op jit(solution)/shard_map/all_gather | solution.py:197
  133.2 0.7 copy-start.14
  133.2 16.8 %copy-start.9 = (bf16[512,512]{1,0:T(8,128)(2,1)S(1)}, bf16[512,512]{1,0:T(8,128)(2,1)}, u32[]{:S(2)}) copy-start(bf16[512,512]{1,0:T(8,128)(2,1)} %param.18) | copy-start | bytes 1572868
  133.3 134.7 %all-gather.14.cloned.1.call-start = ((), (), s32[]{:S(2)}) async-start(), calls=%async_computation.4 | async-start | bytes 2621440 | tf_op jit(solution)/shard_map/all_gather | solution.py:207
  219.6 5.8 %copy-start.3 = (bf16[1024,4096]{1,0:T(8,128)(2,1)S(1)}, bf16[1024,4096]{1,0:T(8,128)(2,1)}, u32[]{:S(2)}) copy-start(bf16[1024,4096]{1,0:T(8,128)(2,1)} %all-gather.12.cloned.1.call-done) | copy-start | bytes 25165828
  225.4 4.1 %copy-start.13 = (bf16[1,256,4096]{2,1,0:T(8,128)(2,1)S(1)}, bf16[1,256,4096]{2,1,0:T(8,128)(2,1)}, u32[]{:S(2)}) copy-start(bf16[1,256,4096]{2,1,0:T(8,128)(2,1)} %param.30) | copy-start | bytes 6291460
  232.8 90.1 %all-gather.10.cloned.1.call-start = ((), (), s32[]{:S(2)}) async-start(), calls=%async_computation.2 | async-start | bytes 5242880 | tf_op jit(solution)/shard_map/all_gather | solution.py:196
  236.0 4.4 %copy-start.6 = (bf16[4,512,256]{2,1,0:T(8,128)(2,1)S(1)}, bf16[4,512,256]{2,1,0:T(8,128)(2,1)}, u32[]{:S(2)}) copy-start(bf16[4,512,256]{2,1,0:T(8,128)(2,1)} %copy.78) | copy-start | bytes 3145732
  246.1 1.6 copy-start.4
  246.1 1.8 copy-start.8
  246.1 1.8 copy-start.11
  273.3 5.5 %copy-start.12 = (f32[256,2]{0,1:T(2,128)S(1)}, f32[256,2]{0,1:T(2,128)}, u32[]{:S(2)}) copy-start(f32[256,2]{0,1:T(2,128)} %param.28) | copy-start | bytes 6148
  273.3 59.7 %all-to-all-start.1 = ((bf16[8,128,1024]{2,1,0:T(8,128)(2,1)}), bf16[8,128,1024]{2,1,0:T(8,128)(2,1)}, u32[]{:S(2)}, u32[]{:S(2)}) async-start(bf16[8,128,1024]{2,1,0:T(8,128)(2,1)} %bitcast.232), calls=%async_computation.1 | async-start | bytes 4194304 | tf_op jit(solution)/shard_map/all_to_all | solution.py:211
Sparse Core Ops, SparseCore 0:
  40.1 86.1 all-gather.15
  133.4 86.1 all-gather.11
  232.9 35.0 all-gather.13
  270.3 52.5 all-gather.9
where the time goes:
time: 353 us; the launch traced here: 352 us
  blocking collectives  111 us (31%)
  waiting for transfers between devices  107 us (30%)
  other arithmetic  47 us (13%)
  matrix products  34.5 us (10%)
  local copies, waits for them, and re-layouts  32.5 us (9%)
  between operations  14.9 us (4%)
  starting transfers between devices  5.12 us (1%)
    all_to_all x1, blocking collectives, body(): lax.all_to_all(jnp.where(occupied[:, None], jnp.take(expert_input, source...  83.4 us
    all_gather x1, waiting for transfers between devices, body(): token_piece = lax.all_gather(arrived, 'tp', axis=1, tiled=True)  44.2 us
    all_gather x1, waiting for transfers between devices, body(): head_piece = lax.all_gather(mixed_heads, 'tp', axis=1, tiled=True)  44 us
    all_gather x1, waiting for transfers between devices, body(): lax.all_gather(hidden, 'tp', axis=1, tiled=True)  18.4 us
    unnamed x1, blocking collectives  14.3 us
    all_gather x1, blocking collectives, carried_in(): pieces = jax.tree.map(lambda part: lax.all_gather(part, axis), value)  13 us
    dot_general x1, matrix products, body(): jnp.dot(head_piece, mix_weight, preferred_element_type=jnp.float32)  10.1 us
    add x8, other arithmetic, combine(): keep_first[..., None, None] * memory_first  9.38 us
  transfers between devices with their start and end apart: 5, of which 3 were waited for; matrix products, arithmetic and copies ran while one was open for 16% of the time, Pallas kernels for 0%

commit v1 on v0

v1 whole, which is shorter than its diff:
```python
import functools

import jax
import jax.numpy as jnp
from jax import lax
from jax.experimental import pallas as pl
from jax.experimental.pallas import tpu as pltpu
from jax.sharding import PartitionSpec as P

EPSILON = 1e-06
LOG_FLOOR = -1e30
F32 = jnp.float32
BF16 = jnp.bfloat16
GROUPS = 4
PAD = 16


def flip(index, bits):
    place = 1
    while place <= bits:
        if bits & place:
            index = index + place * (1 - 2 * ((index // place) % 2))
        place *= 2
    return index


def dot(left, right, contract=((1,), (0,))):
    return lax.dot_general(left, right, (contract, ((), ())), preferred_element_type=F32)


def kernel(
    ep,
    tp,
    head_count,
    model_width,
    x_ref,
    slot_row_ref,
    slot_col_ref,
    weight_ref,
    a_row_ref,
    a_col_ref,
    cum_col_ref,
    gain_ref,
    q_hbm,
    k_hbm,
    v_hbm,
    og_hbm,
    wg_hbm,
    wu_hbm,
    wd_hbm,
    wm_hbm,
    mix_ref,
    exp_ref,
    q_ref,
    k_ref,
    v_ref,
    og_ref,
    wg_ref,
    wu_ref,
    wd_ref,
    wm_ref,
    slots,
    tok,
    hid,
    outb,
    ret,
    hm,
    local,
    st_in,
    st_out,
    load_sem,
    disp_send,
    disp_recv,
    tok_send,
    tok_recv,
    fwd_send,
    fwd_recv,
    hid_send,
    hid_recv,
    ret_send,
    ret_recv,
    head_send,
    head_recv,
    hfwd_send,
    hfwd_recv,
    st_send,
    st_recv,
):
    me = lax.axis_index("ep")
    mine = lax.axis_index("tp")
    cap = slots.shape[0] // ep
    span = slots.shape[0] // GROUPS
    per = ep // GROUPS
    width = x_ref.shape[1]
    length = q_ref.shape[0]
    qk = q_ref.shape[1] // head_count
    vw = v_ref.shape[1] // head_count
    units = wg_ref.shape[0]
    square = tp == 4

    loads = [
        pltpu.make_async_copy(source, target, load_sem.at[at])
        for at, (source, target) in enumerate(
            [
                (k_hbm, k_ref),
                (v_hbm, v_ref),
                (q_hbm, q_ref),
                (og_hbm, og_ref),
                (wg_hbm, wg_ref),
                (wu_hbm, wu_ref),
                (wd_hbm, wd_ref),
                (wm_hbm, wm_ref),
            ]
        )
    ]
    for load in loads:
        load.start()

    barrier = pltpu.get_barrier_semaphore()
    for i in range(1, ep):
        pl.semaphore_signal(barrier, inc=1, device_id={"ep": flip(me, i)})
    for j in range(1, tp):
        pl.semaphore_signal(barrier, inc=1, device_id={"tp": flip(mine, j)})

    tokens = x_ref.shape[0]

    def pick(group, carry):
        at = group * span
        rows = at + lax.broadcasted_iota(jnp.int32, (span, tokens), 0)
        hit = (rows == slot_row_ref[0:1, :]) | (rows == slot_row_ref[1:2, :])
        chosen = dot(hit.astype(F32).astype(BF16), x_ref[...]).astype(BF16)
        slots[pl.ds(pl.multiple_of(at, span), span), :] = chosen
        return carry

    lax.fori_loop(0, GROUPS, pick, 0)
    pl.semaphore_wait(barrier, ep - 1 + tp - 1)

    def dispatch(i):
        return pltpu.make_async_remote_copy(
            slots.at[pl.ds(i * cap, cap)],
            tok.at[0, pl.ds(i * cap, cap)],
            disp_send.at[i],
            disp_recv.at[i],
            device_id={"ep": flip(me, i)},
        )

    for i in range(1, ep):
        dispatch(i).start()
    tok[0, 0:cap, :] = slots[0:cap, :]

    def spread(group, j):
        return pltpu.make_async_remote_copy(
            tok.at[0, pl.ds(group * span, span)],
            tok.at[j, pl.ds(group * span, span)],
            tok_send.at[group, j],
            tok_recv.at[group, j],
            device_id={"tp": flip(mine, j)},
        )

    half = span // 2

    def onward(group, j):
        part = pl.ds(group * span + (j - 1) * half, half)
        return pltpu.make_async_remote_copy(
            tok.at[j, part],
            tok.at[3, part],
            fwd_send.at[group, j],
            fwd_recv.at[group, j],
            device_id={"tp": flip(mine, 3 - j)},
        )

    direct = (1, 2) if square else tuple(range(1, tp))

    def send_group(group):
        for i in range(max(1, group * per), (group + 1) * per):
            dispatch(i).wait_recv()
        for j in direct:
            spread(group, j).start()

    def relay_group(group):
        if square:
            for j in (1, 2):
                spread(group, j).wait_recv()
                onward(group, j).start()

    def collect_group(group):
        if square:
            for j in (1, 2):
                onward(group, j).wait_recv()
        else:
            for j in direct:
                spread(group, j).wait_recv()

    send_group(0)

    loads[0].wait()
    loads[1].wait()

    def summarise(h, carry):
        keys = k_ref[:, pl.ds(pl.multiple_of(h * qk, qk), qk)]
        values = v_ref[:, pl.ds(pl.multiple_of(h * vw, vw), vw)]
        top = jnp.max(a_row_ref[h], axis=1, keepdims=True)
        weighted = keys.astype(F32) * jnp.exp(a_col_ref[h] - top)
        local[h, 0:qk, :] = dot(weighted.astype(BF16), values, ((0,), (0,)))
        normal = jnp.sum(weighted, axis=0, keepdims=True)
        local[h, qk : qk + 8, 0:qk] = jnp.broadcast_to(normal, (8, qk))
        decay = cum_col_ref[h, length - 1 : length, :]
        local[h, qk + 8 : qk + 16, :] = jnp.broadcast_to(top + decay, (8, vw))
        return carry

    lax.fori_loop(0, head_count, summarise, 0)
    send_group(1)

    def chain(h):
        return pltpu.make_async_remote_copy(
            st_out.at[h],
            st_in.at[h],
            st_send.at[h],
            st_recv.at[h],
            device_id={"ep": me + 1},
        )

    @pl.when(me == 0)
    def _():
        st_in[:, 0 : qk + 8, :] = jnp.zeros((head_count, qk + 8, vw), F32)
        st_in[:, qk + 8 : qk + 16, :] = jnp.full((head_count, 8, vw), LOG_FLOOR, F32)

    for h in range(head_count):

        @pl.when(me > 0)
        def _():
            chain(h).wait_recv()

        decay = cum_col_ref[h, length - 1 : length, :]
        carried_max = st_in[h, qk + 8 : qk + 9, :] + decay
        own_max = local[h, qk + 8 : qk + 9, :]
        new_max = jnp.maximum(carried_max, own_max)
        keep = jnp.exp(carried_max - new_max)
        add = jnp.exp(own_max - new_max)
        st_out[h, 0:qk, :] = keep * st_in[h, 0:qk, :] + add * local[h, 0:qk, :]
        st_out[h, qk : qk + 8, 0:qk] = (
            keep[:, 0:qk] * st_in[h, qk : qk + 8, 0:qk]
            + add[:, 0:qk] * local[h, qk : qk + 8, 0:qk]
        )
        st_out[h, qk : qk + 8, qk:vw] = jnp.zeros((8, vw - qk), F32)
        st_out[h, qk + 8 : qk + 16, :] = jnp.broadcast_to(new_max, (8, vw))

        @pl.when(me < ep - 1)
        def _():
            chain(h).start()

    relay_group(0)
    send_group(2)
    loads[2].wait()
    loads[3].wait()

    def heads(h, carry):
        columns = pl.ds(pl.multiple_of(h * vw, vw), vw)
        queries = q_ref[:, pl.ds(pl.multiple_of(h * qk, qk), qk)]
        keys = k_ref[:, pl.ds(pl.multiple_of(h * qk, qk), qk)]
        scale = qk**-0.5
        causal = lax.broadcasted_iota(jnp.int32, (length, length), 1) <= lax.broadcasted_iota(
            jnp.int32, (length, length), 0
        )
        log_in = jnp.where(causal, a_row_ref[h], -jnp.inf)
        prior_max = st_in[h, qk + 8 : qk + 9, 0:1]
        top = jnp.maximum(prior_max, jnp.max(log_in, axis=1, keepdims=True))
        scores = dot(queries, keys, ((1,), (1,))) * scale * jnp.exp(log_in - top)
        carried = jnp.exp(prior_max - top) * scale
        memory = st_in[h, 0:qk, :]
        high = memory.astype(BF16)
        low = (memory - high.astype(F32)).astype(BF16)
        numerator = carried * (dot(queries, high) + dot(queries, low)) + dot(
            scores.astype(BF16), v_ref[:, columns]
        )
        normal = st_in[h, qk : qk + 1, 0:qk]
        denominator = carried * jnp.sum(
            queries.astype(F32) * normal, axis=1, keepdims=True
        ) + jnp.sum(scores, axis=1, keepdims=True)
        floor = jnp.exp(-(cum_col_ref[h] + top))
        value = numerator / jnp.maximum(jnp.abs(denominator), floor)
        value = value * lax.rsqrt(jnp.mean(value * value, axis=1, keepdims=True) + EPSILON)
        gate = jax.nn.sigmoid(og_ref[:, columns].astype(F32))
        hm[0, :, columns] = (value * gain_ref[:, columns] * gate).astype(BF16)
        return carry

    lax.fori_loop(0, head_count, heads, 0)
    relay_group(1)
    send_group(3)

    loads[4].wait()
    loads[5].wait()

    def expand(group):
        rows = pl.ds(group * span, span)

        gate = jnp.zeros((span, units), F32)
        up = jnp.zeros((span, units), F32)
        squares = jnp.zeros((span, 1), F32)
        for j in range(tp):
            piece = tok[j, rows, :]
            columns = pl.ds(pl.multiple_of(flip(mine, j) * width, width), width)
            gate += dot(piece, wg_ref[:, columns], ((1,), (1,)))
            up += dot(piece, wu_ref[:, columns], ((1,), (1,)))
            wide = piece.astype(F32)
            squares += jnp.sum(wide * wide, axis=1, keepdims=True)
        inverse = lax.rsqrt(squares / model_width + EPSILON)
        hid[0, rows, :] = (jax.nn.silu(gate * inverse) * (up * inverse)).astype(BF16)

    def share(group, j):
        return pltpu.make_async_remote_copy(
            hid.at[0, pl.ds(group * span, span)],
            hid.at[j, pl.ds(group * span, span)],
            hid_send.at[group, j],
            hid_recv.at[group, j],
            device_id={"tp": flip(mine, j)},
        )

    for group in range(GROUPS):
        if group + 2 < GROUPS:
            relay_group(group + 2)
        collect_group(group)
        expand(group)
        for j in range(1, tp):
            share(group, j).start()

    def head_spread(j):
        return pltpu.make_async_remote_copy(
            hm.at[0], hm.at[j], head_send.at[j], head_recv.at[j], device_id={"tp": flip(mine, j)}
        )

    def head_onward(j):
        part = pl.ds((j - 1) * (length // 2), length // 2)
        return pltpu.make_async_remote_copy(
            hm.at[j, part],
            hm.at[3, part],
            hfwd_send.at[j],
            hfwd_recv.at[j],
            device_id={"tp": flip(mine, 3 - j)},
        )

    for j in direct:
        head_spread(j).start()

    def give_back(i):
        return pltpu.make_async_remote_copy(
            outb.at[pl.ds(i * cap, cap)],
            ret.at[pl.ds(i * cap, cap)],
            ret_send.at[i],
            ret_recv.at[i],
            device_id={"ep": flip(me, i)},
        )

    loads[6].wait()
    for group in range(GROUPS - 1, -1, -1):
        rows = pl.ds(group * span, span)
        for j in range(1, tp):
            share(group, j).wait_recv()
        total = jnp.zeros((span, width), F32)
        for j in range(tp):
            at = pl.ds(pl.multiple_of(flip(mine, j) * units, units), units)
            total += dot(hid[j, rows, :], wd_ref[at, :])
        outb[rows, :] = total.astype(BF16)
        for i in range(max(1, group * per), (group + 1) * per):
            give_back(i).start()
    ret[0:cap, :] = outb[0:cap, :]

    loads[7].wait()
    if square:
        for j in (1, 2):
            head_spread(j).wait_recv()
            head_onward(j).start()
    tile = length // 2

    def mix_with(blocks):
        def step(at, carry):
            rows = pl.ds(pl.multiple_of(at * tile, tile), tile)
            total = jnp.zeros((tile, width), F32)
            for j in blocks:
                inputs = pl.ds(pl.multiple_of(flip(mine, j) * width, width), width)
                total += dot(hm[j, rows, :], wm_ref[inputs, :])
            mix_ref[rows, :] = total.astype(BF16)
            return carry

        lax.fori_loop(0, 2, step, 0)

    if square:
        for j in (1, 2):
            head_onward(j).wait_recv()
    else:
        for j in direct:
            head_spread(j).wait_recv()
    mix_with(range(tp))

    for i in range(1, ep):
        give_back(i).wait_recv()
    places = lax.broadcasted_iota(jnp.int32, (tokens, slots.shape[0]), 1)
    total = jnp.zeros((tokens, width), F32)
    for route in range(weight_ref.shape[1]):
        hit = places == slot_col_ref[:, route : route + 1]
        picked = dot(hit.astype(F32).astype(BF16), ret[...])
        total += picked * weight_ref[:, route : route + 1]
    exp_ref[...] = total.astype(BF16)

    for i in range(1, ep):
        dispatch(i).wait_send()
        give_back(i).wait_send()
    for group in range(GROUPS):
        for j in direct:
            spread(group, j).wait_send()
        for j in range(1, tp):
            share(group, j).wait_send()
        if square:
            for j in (1, 2):
                onward(group, j).wait_send()
    for j in direct:
        head_spread(j).wait_send()
    if square:
        for j in (1, 2):
            head_onward(j).wait_send()
    for h in range(head_count):

        @pl.when(me < ep - 1)
        def _():
            chain(h).wait_send()


def body(
    query_rows,
    key_rows,
    value_rows,
    in_gate,
    forget_gate,
    out_gate,
    head_gain,
    mix_weight,
    expert_input,
    routes,
    route_weight,
    gate_weight,
    up_weight,
    down_weight,
):
    ep, tp = lax.axis_size("ep"), lax.axis_size("tp")
    head_count, length = in_gate.shape
    token_count, fanout = routes.shape
    width = expert_input.shape[1]
    units = gate_weight.shape[1]
    capacity = 2 * token_count * fanout // ep
    slot_count = ep * capacity
    qk = query_rows.shape[1] // head_count
    vw = value_rows.shape[1] // head_count

    earlier = jnp.tril(jnp.ones((length, length), F32))
    cumulative = jnp.einsum(
        "hs,ts->ht", jax.nn.log_sigmoid(forget_gate), earlier, precision=lax.Precision.HIGHEST
    )
    shifted = in_gate - cumulative

    me = lax.axis_index("ep")
    turned = routes ^ me
    experts = jnp.arange(ep, dtype=jnp.int32)
    named = turned[:, :, None] == experts
    any_named = jnp.any(named, axis=1)
    before = jnp.dot(
        jnp.tril(jnp.ones((token_count, token_count), BF16), -1),
        any_named.astype(BF16),
        preferred_element_type=F32,
    ).astype(jnp.int32)
    places = experts * capacity + before
    slot_col = jnp.sum(jnp.where(named, places[:, None, :], 0), axis=2)
    slot_row = slot_col.T

    vmem = pl.BlockSpec(memory_space=pltpu.VMEM)
    anywhere = pl.BlockSpec(memory_space=pl.ANY)
    dma = pltpu.SemaphoreType.DMA
    gate_local, up_local, down_local = gate_weight[0], up_weight[0], down_weight[0]
    big = (query_rows, key_rows, value_rows, out_gate, gate_local, up_local, down_local, mix_weight)
    state = (head_count, qk + PAD, vw)
    return pl.pallas_call(
        functools.partial(kernel, ep, tp, head_count, mix_weight.shape[0]),
        out_shape=(
            jax.ShapeDtypeStruct((length, width), BF16),
            jax.ShapeDtypeStruct((token_count, width), BF16),
        ),
        in_specs=[vmem] * 8 + [anywhere] * 8,
        out_specs=(vmem, vmem),
        scratch_shapes=[pltpu.VMEM(array.shape, array.dtype) for array in big]
        + [
            pltpu.VMEM((slot_count, width), BF16),
            pltpu.VMEM((tp, slot_count, width), BF16),
            pltpu.VMEM((tp, slot_count, units), BF16),
            pltpu.VMEM((slot_count, width), BF16),
            pltpu.VMEM((slot_count, width), BF16),
            pltpu.VMEM((tp, length, width), BF16),
            pltpu.VMEM(state, F32),
            pltpu.VMEM(state, F32),
            pltpu.VMEM(state, F32),
            dma((8,)),
            dma((ep,)),
            dma((ep,)),
            dma((GROUPS, tp)),
            dma((GROUPS, tp)),
            dma((GROUPS, 4)),
            dma((GROUPS, 4)),
            dma((GROUPS, tp)),
            dma((GROUPS, tp)),
            dma((ep,)),
            dma((ep,)),
            dma((tp,)),
            dma((tp,)),
            dma((4,)),
            dma((4,)),
            dma((head_count,)),
            dma((head_count,)),
        ],
        compiler_params=pltpu.CompilerParams(
            collective_id=0, has_side_effects=True, vmem_limit_bytes=64000 * 1024
        ),
    )(
        expert_input,
        slot_row,
        slot_col,
        route_weight,
        shifted[:, None, :],
        shifted[:, :, None],
        cumulative[:, :, None],
        head_gain[None, :],
        *big,
    )


def solution(mesh):
    in_specs = (
        P("ep", "tp"),
        P("ep", "tp"),
        P("ep", "tp"),
        P("tp", "ep"),
        P("tp", "ep"),
        P("ep", "tp"),
        P("tp"),
        P(None, "tp"),
        P("ep", "tp"),
        P("ep", None),
        P("ep", None),
        P("ep", "tp", None),
        P("ep", "tp", None),
        P("ep", None, "tp"),
    )
    out_specs = (P("ep", "tp"), P("ep", "tp"))
    return jax.shard_map(body, mesh=mesh, in_specs=in_specs, out_specs=out_specs, check_vma=False)
```

time: 353 us -> 195 us (0.55)
  Pallas kernels: 0 us -> 183 us
  blocking collectives: 111 us -> 0 us
  waiting for transfers between devices: 107 us -> 0 us
  other arithmetic: 47 us -> 0.75 us
  matrix products: 34.5 us -> 1.59 us
  local copies, waits for them, and re-layouts: 32.5 us -> 8.72 us
  between operations: 14.9 us -> 0.68 us
  starting transfers between devices: 5.12 us -> 0 us
    pallas_call x0 -> x1, Pallas kernels: none -> 183 us  [body(): pl.pallas_call(functools.partial(kernel, ep, tp, head_count, mix_weight.s...]
    all_gather x4 -> x0, waiting for transfers between devices: 107 us -> none  [the longest x1 44.2 us: body(): token_piece = lax.all_gather(arrived, 'tp', axis=1, tiled=True)]
    all_to_all x1 -> x0, blocking collectives: 83.4 us -> none  [body(): lax.all_to_all(jnp.where(occupied[:, None], jnp.take(expert_input, source...]
    dot_general x9 -> x2, matrix products: 34.5 us -> 1.59 us  [the longest x1 1.35 us: body(): jnp.einsum('hs,ts->ht', jax.nn.log_sigmoid(forget_gate), earlier, precisi...]
    unnamed x1 -> x0, blocking collectives: 14.3 us -> none
    all_gather x1 -> x0, blocking collectives: 13 us -> none  [carried_in(): pieces = jax.tree.map(lambda part: lax.all_gather(part, axis), value)]
    reduce_sum x5 -> x1, other arithmetic: 12.6 us -> 0.04 us  [body(): slot_col = jnp.sum(jnp.where(named, places[:, None, :], 0), axis=2)]
    gather x3 -> x0, local copies, waits for them, and re-layouts: 11.2 us -> none  [the longest x2 5.83 us: body(): jnp.take(returned_rows, target, axis=0).reshape(token_count, fanout, -1)]
  transfers between devices with their start and end apart: 5 -> 0, of which waited for: 3 -> 0; matrix products, arithmetic and copies ran while one was open for 16% -> 0% of each run, Pallas kernels for 0% -> 0%
where the time goes in v1:
time: 195 us
  Pallas kernels  183 us (94%)
  local copies, waits for them, and re-layouts  8.72 us (4%)
    pallas_call x1, Pallas kernels, body(): pl.pallas_call(functools.partial(kernel, ep, tp, head_count, mix_weight.s...  183 us
    unnamed x7, local copies, waits for them, and re-layouts  4.58 us

profile of v1, /device:TPU:0, one launch (start us, length us, event | category | flops | bytes accessed | tf_op | source)
XLA Modules:
  0.0 195.1 jit_solution(17003669751089200635)
XLA Ops:
  0.7 0.7 broadcast_xor_fusion
  1.4 0.2 fusion
  1.6 0.0 copy-start.1
  1.6 1.4 fusion.25
  3.0 0.6 broadcast_in_dim.48.a_row_ref
  3.6 0.8 copy.27.slot_col_ref
  4.4 1.5 copy.28.weight_ref
  5.9 1.4 copy.30.cum_col_ref
  7.2 1.3 copy.29.a_col_ref
  8.6 0.0 copy-done.1
  8.6 183.4 %shard_map.149 = (bf16[512,1024]{1,0:T(8,128)(2,1)}, bf16[256,1024]{1,0:T(8,128)(2,1)}) custom-call(bf16[256,1024]{1,0:T(8,128)(2,1)} %x_ref.1, s32[2,256]{1,0:T(2,128)} %bitcast.12, s32[256,2]{1,0:T(8,128)} %copy.27.slot_col_ref, f32[256,2]{1,0:T(8,128)} %copy.28.weight_ref, f32[4,1,512]{2,1,0:T(1,128)} %broadcast_in_dim.48.a_row_ref, ...), custom_call_target="tpu_custom_call" | custom-call | tf_op jit(solution)/shard_map/pallas_call | solution.py:480
  192.0 0.0 copy-start
  192.0 2.3 %copy.33 = bf16[512,1024]{1,0:T(8,128)(2,1)} copy(bf16[512,1024]{1,0:T(8,128)(2,1)} %get-tuple-element.6) | data formatting | bytes 2097152
  194.3 0.0 copy-done
  194.3 0.8 copy.34
  (4 shorter events, 0.1 us)
Async XLA Ops:
  1.6 7.0 %copy-start.1 = (s32[256,2]{0,1:T(2,128)}, s32[256,2]{0,1:T(2,128)S(1)}, u32[]{:S(2)}) copy-start(s32[256,2]{0,1:T(2,128)S(1)} %select_reduce_fusion) | copy-start | bytes 6148
  192.0 2.3 %copy-start = (bf16[256,1024]{1,0:T(8,128)(2,1)S(1)}, bf16[256,1024]{1,0:T(8,128)(2,1)}, u32[]{:S(2)}) copy-start(bf16[256,1024]{1,0:T(8,128)(2,1)} %get-tuple-element.7) | copy-start | bytes 1572868

commit v2 on v1

--- a/solution.py
+++ b/solution.py
@@ -28,6 +28,14 @@
     return lax.dot_general(left, right, (contract, ((), ())), preferred_element_type=F32)
 
 
+def upright(row):
+    size = row.shape[1]
+    own = lax.broadcasted_iota(jnp.int32, (size, size), 0) == lax.broadcasted_iota(
+        jnp.int32, (size, size), 1
+    )
+    return jnp.sum(jnp.where(own, row, jnp.zeros((), row.dtype)), axis=1, keepdims=True)
+
+
 def kernel(
     ep,
     tp,
@@ -35,11 +43,9 @@
     model_width,
     x_ref,
     slot_row_ref,
-    slot_col_ref,
     weight_ref,
-    a_row_ref,
-    a_col_ref,
-    cum_col_ref,
+    a_ref,
+    cum_ref,
     gain_ref,
     q_hbm,
     k_hbm,
@@ -144,8 +150,19 @@
             device_id={"ep": flip(me, i)},
         )
 
-    for i in range(1, ep):
-        dispatch(i).start()
+    near = per
+    far = [i for i in range(2 * per, ep)] + [i for i in range(per, 2 * per)]
+    waits_for_chain = me % 2 == 1
+    for i in [i for i in range(1, per)] + far:
+        if i < near:
+            dispatch(i).start()
+        else:
+            held = waits_for_chain & (flip(me, i) > me)
+
+            @pl.when(jnp.logical_not(held))
+            def _():
+                dispatch(i).start()
+
     tok[0, 0:cap, :] = slots[0:cap, :]
 
     def spread(group, j):
@@ -199,17 +216,21 @@
     def summarise(h, carry):
         keys = k_ref[:, pl.ds(pl.multiple_of(h * qk, qk), qk)]
         values = v_ref[:, pl.ds(pl.multiple_of(h * vw, vw), vw)]
-        top = jnp.max(a_row_ref[h], axis=1, keepdims=True)
-        weighted = keys.astype(F32) * jnp.exp(a_col_ref[h] - top)
+        log_in = a_ref[pl.ds(h, 1), :]
+        top = jnp.max(log_in, axis=1, keepdims=True)
+        weighted = keys.astype(F32) * jnp.exp(upright(log_in) - top)
         local[h, 0:qk, :] = dot(weighted.astype(BF16), values, ((0,), (0,)))
         normal = jnp.sum(weighted, axis=0, keepdims=True)
         local[h, qk : qk + 8, 0:qk] = jnp.broadcast_to(normal, (8, qk))
-        decay = cum_col_ref[h, length - 1 : length, :]
+        decay = cum_ref[pl.ds(h, 1), :][:, length - 1 : length]
         local[h, qk + 8 : qk + 16, :] = jnp.broadcast_to(top + decay, (8, vw))
         return carry
 
     lax.fori_loop(0, head_count, summarise, 0)
-    send_group(1)
+
+    @pl.when(me >= ep // 2)
+    def _():
+        relay_group(0)
 
     def chain(h):
         return pltpu.make_async_remote_copy(
@@ -231,7 +252,7 @@
         def _():
             chain(h).wait_recv()
 
-        decay = cum_col_ref[h, length - 1 : length, :]
+        decay = cum_ref[h : h + 1, length - 1 : length]
         carried_max = st_in[h, qk + 8 : qk + 9, :] + decay
         own_max = local[h, qk + 8 : qk + 9, :]
         new_max = jnp.maximum(carried_max, own_max)
@@ -249,8 +270,19 @@
         def _():
             chain(h).start()
 
-    relay_group(0)
+    for i in far:
+        held = waits_for_chain & (flip(me, i) > me)
+
+        @pl.when(held)
+        def _():
+            dispatch(i).start()
+
+    @pl.when(me < ep // 2)
+    def _():
+        relay_group(0)
+
     send_group(2)
+
     loads[2].wait()
     loads[3].wait()
 
@@ -262,7 +294,7 @@
         causal = lax.broadcasted_iota(jnp.int32, (length, length), 1) <= lax.broadcasted_iota(
             jnp.int32, (length, length), 0
         )
-        log_in = jnp.where(causal, a_row_ref[h], -jnp.inf)
+        log_in = jnp.where(causal, a_ref[pl.ds(h, 1), :], -jnp.inf)
         prior_max = st_in[h, qk + 8 : qk + 9, 0:1]
         top = jnp.maximum(prior_max, jnp.max(log_in, axis=1, keepdims=True))
         scores = dot(queries, keys, ((1,), (1,))) * scale * jnp.exp(log_in - top)
@@ -277,7 +309,7 @@
         denominator = carried * jnp.sum(
             queries.astype(F32) * normal, axis=1, keepdims=True
         ) + jnp.sum(scores, axis=1, keepdims=True)
-        floor = jnp.exp(-(cum_col_ref[h] + top))
+        floor = jnp.exp(-(upright(cum_ref[pl.ds(h, 1), :]) + top))
         value = numerator / jnp.maximum(jnp.abs(denominator), floor)
         value = value * lax.rsqrt(jnp.mean(value * value, axis=1, keepdims=True) + EPSILON)
         gate = jax.nn.sigmoid(og_ref[:, columns].astype(F32))
@@ -285,8 +317,7 @@
         return carry
 
     lax.fori_loop(0, head_count, heads, 0)
-    relay_group(1)
-    send_group(3)
+    relay_group(2)
 
     loads[4].wait()
     loads[5].wait()
@@ -316,32 +347,6 @@
             device_id={"tp": flip(mine, j)},
         )
 
-    for group in range(GROUPS):
-        if group + 2 < GROUPS:
-            relay_group(group + 2)
-        collect_group(group)
-        expand(group)
-        for j in range(1, tp):
-            share(group, j).start()
-
-    def head_spread(j):
-        return pltpu.make_async_remote_copy(
-            hm.at[0], hm.at[j], head_send.at[j], head_recv.at[j], device_id={"tp": flip(mine, j)}
-        )
-
-    def head_onward(j):
-        part = pl.ds((j - 1) * (length // 2), length // 2)
-        return pltpu.make_async_remote_copy(
-            hm.at[j, part],
-            hm.at[3, part],
-            hfwd_send.at[j],
-            hfwd_recv.at[j],
-            device_id={"tp": flip(mine, 3 - j)},
-        )
-
-    for j in direct:
-        head_spread(j).start()
-
     def give_back(i):
         return pltpu.make_async_remote_copy(
             outb.at[pl.ds(i * cap, cap)],
@@ -351,8 +356,7 @@
             device_id={"ep": flip(me, i)},
         )
 
-    loads[6].wait()
-    for group in range(GROUPS - 1, -1, -1):
+    def contract(group):
         rows = pl.ds(group * span, span)
         for j in range(1, tp):
             share(group, j).wait_recv()
@@ -363,44 +367,88 @@
         outb[rows, :] = total.astype(BF16)
         for i in range(max(1, group * per), (group + 1) * per):
             give_back(i).start()
+
+    tile = length // 2
+
+    def head_spread(part, j):
+        rows = pl.ds(part * tile, tile)
+        return pltpu.make_async_remote_copy(
+            hm.at[0, rows],
+            hm.at[j, rows],
+            head_send.at[part, j],
+            head_recv.at[part, j],
+            device_id={"tp": flip(mine, j)},
+        )
+
+    def head_onward(part, j):
+        rows = pl.ds(part * tile + (j - 1) * (tile // 2), tile // 2)
+        return pltpu.make_async_remote_copy(
+            hm.at[j, rows],
+            hm.at[3, rows],
+            hfwd_send.at[part, j],
+            hfwd_recv.at[part, j],
+            device_id={"tp": flip(mine, 3 - j)},
+        )
+
+    def expand_and_share(group):
+        collect_group(group)
+        expand(group)
+        for j in range(1, tp):
+            share(group, j).start()
+
+    def head_relay(part):
+        if square:
+            for j in (1, 2):
+                head_spread(part, j).wait_recv()
+                head_onward(part, j).start()
+
+    def mix(part):
+        rows = pl.ds(part * tile, tile)
+        for j in range(1, tp):
+            if not square:
+                head_spread(part, j).wait_recv()
+            elif j < 3:
+                head_onward(part, j).wait_recv()
+        total = jnp.zeros((tile, width), F32)
+        for j in range(tp):
+            inputs = pl.ds(pl.multiple_of(flip(mine, j) * width, width), width)
+            total += dot(hm[j, rows, :], wm_ref[inputs, :])
+        mix_ref[rows, :] = total.astype(BF16)
+
+    for j in direct:
+        head_spread(0, j).start()
+    send_group(3)
+    loads[6].wait()
+    loads[7].wait()
+    expand_and_share(0)
+    relay_group(3)
+    send_group(1)
+    expand_and_share(2)
+    contract(0)
     ret[0:cap, :] = outb[0:cap, :]
-
-    loads[7].wait()
-    if square:
-        for j in (1, 2):
-            head_spread(j).wait_recv()
-            head_onward(j).start()
-    tile = length // 2
-
-    def mix_with(blocks):
-        def step(at, carry):
-            rows = pl.ds(pl.multiple_of(at * tile, tile), tile)
-            total = jnp.zeros((tile, width), F32)
-            for j in blocks:
-                inputs = pl.ds(pl.multiple_of(flip(mine, j) * width, width), width)
-                total += dot(hm[j, rows, :], wm_ref[inputs, :])
-            mix_ref[rows, :] = total.astype(BF16)
-            return carry
-
-        lax.fori_loop(0, 2, step, 0)
-
-    if square:
-        for j in (1, 2):
-            head_onward(j).wait_recv()
-    else:
-        for j in direct:
-            head_spread(j).wait_recv()
-    mix_with(range(tp))
+    relay_group(1)
+    head_relay(0)
+    expand_and_share(3)
+    contract(2)
+    expand_and_share(1)
+    for j in direct:
+        head_spread(1, j).start()
+    contract(3)
+    mix(0)
+    contract(1)
+    head_relay(1)
 
     for i in range(1, ep):
         give_back(i).wait_recv()
-    places = lax.broadcasted_iota(jnp.int32, (tokens, slots.shape[0]), 1)
+    places = lax.broadcasted_iota(jnp.int32, (slots.shape[0], tokens), 0)
     total = jnp.zeros((tokens, width), F32)
-    for route in range(weight_ref.shape[1]):
-        hit = places == slot_col_ref[:, route : route + 1]
-        picked = dot(hit.astype(F32).astype(BF16), ret[...])
-        total += picked * weight_ref[:, route : route + 1]
+    for route in range(weight_ref.shape[0]):
+        hit = places == slot_row_ref[route : route + 1, :]
+        picked = dot(hit.astype(F32).astype(BF16), ret[...], ((0,), (0,)))
+        total += picked * upright(weight_ref[route : route + 1, :])
     exp_ref[...] = total.astype(BF16)
+
+    mix(1)
 
     for i in range(1, ep):
         dispatch(i).wait_send()
@@ -413,11 +461,12 @@
         if square:
             for j in (1, 2):
                 onward(group, j).wait_send()
-    for j in direct:
-        head_spread(j).wait_send()
-    if square:
-        for j in (1, 2):
-            head_onward(j).wait_send()
+    for part in range(2):
+        for j in direct:
+            head_spread(part, j).wait_send()
+        if square:
+            for j in (1, 2):
+                head_onward(part, j).wait_send()
     for h in range(head_count):
 
         @pl.when(me < ep - 1)
@@ -468,8 +517,7 @@
         preferred_element_type=F32,
     ).astype(jnp.int32)
     places = experts * capacity + before
-    slot_col = jnp.sum(jnp.where(named, places[:, None, :], 0), axis=2)
-    slot_row = slot_col.T
+    slot_row = jnp.sum(jnp.where(named, places[:, None, :], 0), axis=2).T
 
     vmem = pl.BlockSpec(memory_space=pltpu.VMEM)
     anywhere = pl.BlockSpec(memory_space=pl.ANY)
@@ -483,7 +531,7 @@
             jax.ShapeDtypeStruct((length, width), BF16),
             jax.ShapeDtypeStruct((token_count, width), BF16),
         ),
-        in_specs=[vmem] * 8 + [anywhere] * 8,
+        in_specs=[vmem] * 6 + [anywhere] * 8,
         out_specs=(vmem, vmem),
         scratch_shapes=[pltpu.VMEM(array.shape, array.dtype) for array in big]
         + [
@@ -507,10 +555,10 @@
             dma((GROUPS, tp)),
             dma((ep,)),
             dma((ep,)),
-            dma((tp,)),
-            dma((tp,)),
-            dma((4,)),
-            dma((4,)),
+            dma((2, tp)),
+            dma((2, tp)),
+            dma((2, 4)),
+            dma((2, 4)),
             dma((head_count,)),
             dma((head_count,)),
         ],
@@ -520,11 +568,9 @@
     )(
         expert_input,
         slot_row,
-        slot_col,
-        route_weight,
-        shifted[:, None, :],
-        shifted[:, :, None],
-        cumulative[:, :, None],
+        route_weight.T,
+        shifted,
+        cumulative,
         head_gain[None, :],
         *big,
     )

time: 195 us -> 183 us (0.938)
  the two profiles are of different devices: /device:TPU:0 before, /device:TPU:17 now
where the time goes in v2:
time: 183 us; the launch traced here: 182 us
  Pallas kernels  175 us (96%)
  local copies, waits for them, and re-layouts  3.12 us (2%)
  matrix products  2.21 us (1%)
    pallas_call x1, Pallas kernels, body(): pl.pallas_call(functools.partial(kernel, ep, tp, head_count, mix_weight.s...  175 us

profile of v2, /device:TPU:17, one launch (start us, length us, event | category | flops | bytes accessed | tf_op | source)
XLA Modules:
  0.0 182.5 jit_solution(2836001267998048709)
XLA Ops:
  0.7 0.7 broadcast_xor_fusion
  1.4 0.2 fusion
  1.6 0.6 select_reduce_fusion
  2.2 2.0 %fusion.25 = (f32[4,512]{1,0:T(4,128)}, f32[4,512]{1,0:T(4,128)}) fusion(f32[4,512]{1,0:T(4,128)} %param.17, f32[4,512]{1,0:T(4,128)} %param.18), kind=kOutput, calls=%fused_computation.32 | convolution fusion | flops 13125632 | bytes 32768 | tf_op jit(solution)/shard_map/hs,ts->ht/dot_general | solution.py:504
  4.2 175.2 %shard_map.149 = (bf16[512,1024]{1,0:T(8,128)(2,1)}, bf16[256,1024]{1,0:T(8,128)(2,1)}) custom-call(bf16[256,1024]{1,0:T(8,128)(2,1)} %x_ref.1, s32[2,256]{1,0:T(2,128)} %bitcast.10, f32[2,256]{1,0:T(2,128)} %bitcast.12, f32[4,512]{1,0:T(4,128)} %get-tuple-element.2.a_ref, f32[4,512]{1,0:T(4,128)} %get-tuple-element.3.cum_ref, f32[1,1024]{1,0:T(1,128)} %bitcast.11, ...), custom_call_target="tpu_custom_call" | custom-call | tf_op jit(solution)/shard_map/pallas_call | solution.py:528
  179.4 0.0 copy-start
  179.4 2.3 %copy.20 = bf16[512,1024]{1,0:T(8,128)(2,1)} copy(bf16[512,1024]{1,0:T(8,128)(2,1)} %get-tuple-element.6) | data formatting | bytes 2097152
  181.7 0.0 copy-done
  181.7 0.8 copy.21
  (3 shorter events, 0.0 us)
Async XLA Ops:
  179.4 2.3 %copy-start = (bf16[256,1024]{1,0:T(8,128)(2,1)S(1)}, bf16[256,1024]{1,0:T(8,128)(2,1)}, u32[]{:S(2)}) copy-start(bf16[256,1024]{1,0:T(8,128)(2,1)} %get-tuple-element.7) | copy-start | bytes 1572868

commit v3 on v2

--- a/solution.py
+++ b/solution.py
@@ -150,10 +150,9 @@
             device_id={"ep": flip(me, i)},
         )
 
-    near = per
-    far = [i for i in range(2 * per, ep)] + [i for i in range(per, 2 * per)]
+    near = max(2, 2 * per)
     waits_for_chain = me % 2 == 1
-    for i in [i for i in range(1, per)] + far:
+    for i in range(1, ep):
         if i < near:
             dispatch(i).start()
         else:
@@ -230,6 +229,7 @@
 
     @pl.when(me >= ep // 2)
     def _():
+        send_group(1)
         relay_group(0)
 
     def chain(h):
@@ -270,7 +270,7 @@
         def _():
             chain(h).start()
 
-    for i in far:
+    for i in range(near, ep):
         held = waits_for_chain & (flip(me, i) > me)
 
         @pl.when(held)
@@ -279,9 +279,8 @@
 
     @pl.when(me < ep // 2)
     def _():
+        send_group(1)
         relay_group(0)
-
-    send_group(2)
 
     loads[2].wait()
     loads[3].wait()
@@ -316,8 +315,10 @@
         hm[0, :, columns] = (value * gain_ref[:, columns] * gate).astype(BF16)
         return carry
 
-    lax.fori_loop(0, head_count, heads, 0)
-    relay_group(2)
+    lax.fori_loop(0, head_count // 2, heads, 0)
+    relay_group(1)
+    send_group(2)
+    lax.fori_loop(head_count // 2, head_count, heads, 0)
 
     loads[4].wait()
     loads[5].wait()
@@ -396,8 +397,28 @@
         for j in range(1, tp):
             share(group, j).start()
 
-    def head_relay(part):
-        if square:
+    loads[6].wait()
+    for group in range(GROUPS):
+        if group > 1:
+            if group + 1 < GROUPS:
+                relay_group(group + 1)
+        expand_and_share(group)
+        if group == 0:
+            for later in range(3, GROUPS):
+                send_group(later)
+            relay_group(2)
+        elif group < GROUPS - 1:
+            contract(group - 1)
+    for part in range(2):
+        for j in direct:
+            head_spread(part, j).start()
+    contract(GROUPS - 2)
+    contract(GROUPS - 1)
+    ret[0:cap, :] = outb[0:cap, :]
+
+    loads[7].wait()
+    if square:
+        for part in range(2):
             for j in (1, 2):
                 head_spread(part, j).wait_recv()
                 head_onward(part, j).start()
@@ -415,28 +436,7 @@
             total += dot(hm[j, rows, :], wm_ref[inputs, :])
         mix_ref[rows, :] = total.astype(BF16)
 
-    for j in direct:
-        head_spread(0, j).start()
-    send_group(3)
-    loads[6].wait()
-    loads[7].wait()
-    expand_and_share(0)
-    relay_group(3)
-    send_group(1)
-    expand_and_share(2)
-    contract(0)
-    ret[0:cap, :] = outb[0:cap, :]
-    relay_group(1)
-    head_relay(0)
-    expand_and_share(3)
-    contract(2)
-    expand_and_share(1)
-    for j in direct:
-        head_spread(1, j).start()
-    contract(3)
     mix(0)
-    contract(1)
-    head_relay(1)
 
     for i in range(1, ep):
         give_back(i).wait_recv()

time: 183 us -> 174 us (0.951)
  the two profiles are of different devices: /device:TPU:17 before, /device:TPU:8 now
where the time goes in v3:
time: 174 us; the launch traced here: 173 us
  Pallas kernels  166 us (95%)
  local copies, waits for them, and re-layouts  3.12 us (2%)
  matrix products  2.21 us (1%)
    pallas_call x1, Pallas kernels, body(): pl.pallas_call(functools.partial(kernel, ep, tp, head_count, mix_weight.s...  166 us

profile of v3, /device:TPU:8, one launch (start us, length us, event | category | flops | bytes accessed | tf_op | source)
XLA Modules:
  0.0 173.2 jit_solution(6788261632074362285)
XLA Ops:
  0.7 0.7 broadcast_xor_fusion
  1.4 0.2 fusion
  1.6 0.6 select_reduce_fusion
  2.2 2.0 %fusion.25 = (f32[4,512]{1,0:T(4,128)}, f32[4,512]{1,0:T(4,128)}) fusion(f32[4,512]{1,0:T(4,128)} %param.17, f32[4,512]{1,0:T(4,128)} %param.18), kind=kOutput, calls=%fused_computation.32 | convolution fusion | flops 13125632 | bytes 32768 | tf_op jit(solution)/shard_map/hs,ts->ht/dot_general | solution.py:504
  4.2 165.9 %shard_map.149 = (bf16[512,1024]{1,0:T(8,128)(2,1)}, bf16[256,1024]{1,0:T(8,128)(2,1)}) custom-call(bf16[256,1024]{1,0:T(8,128)(2,1)} %x_ref.1, s32[2,256]{1,0:T(2,128)} %bitcast.10, f32[2,256]{1,0:T(2,128)} %bitcast.12, f32[4,512]{1,0:T(4,128)} %get-tuple-element.2.a_ref, f32[4,512]{1,0:T(4,128)} %get-tuple-element.3.cum_ref, f32[1,1024]{1,0:T(1,128)} %bitcast.11, ...), custom_call_target="tpu_custom_call" | custom-call | tf_op jit(solution)/shard_map/pallas_call | solution.py:528
  170.1 0.0 copy-start
  170.1 2.3 %copy.20 = bf16[512,1024]{1,0:T(8,128)(2,1)} copy(bf16[512,1024]{1,0:T(8,128)(2,1)} %get-tuple-element.6) | data formatting | bytes 2097152
  172.5 0.0 copy-done
  172.5 0.8 copy.21
  (3 shorter events, 0.0 us)
Async XLA Ops:
  170.1 2.3 %copy-start = (bf16[256,1024]{1,0:T(8,128)(2,1)S(1)}, bf16[256,1024]{1,0:T(8,128)(2,1)}, u32[]{:S(2)}) copy-start(bf16[256,1024]{1,0:T(8,128)(2,1)} %get-tuple-element.7) | copy-start | bytes 1572868
